TPU v7x, 32 devices: a whole 2x2x4 slice. The times are simulated.
32 devices in a mesh: sp: 16 (over z, y, x), tp: 2 (over core).
Axes of the slice: x: 2, y: 2, z: 4, core: 2. Of those that a mesh axis runs over, the one named last changes fastest.
Arguments:
- queries: bfloat16 [2048, 768], P('sp', 'tp'), may hold values from -6 to 6
- latents: bfloat16 [2048, 512], P('sp'), may hold values from -6 to 6
- rot_key: bfloat16 [2048, 32], P('sp'), may hold values from -6 to 6
- kv_weight: bfloat16 [512, 1024], P(None, 'tp'), may hold values from -0.25 to 0.25
- log_sums: float32 [2048, 8], P('sp', 'tp'), may hold values from 4 to 14, as said below
- outputs: bfloat16 [2048, 512], P('sp', 'tp'), may hold values from -4 to 4
- out_grad: bfloat16 [2048, 512], P('sp', 'tp'), may hold values from -96 to 96
Outputs:
- query_grad: bfloat16 [2048, 768], P('sp', 'tp')
- key_grad: bfloat16 [2048, 512], P('sp', 'tp')
- value_grad: bfloat16 [2048, 512], P('sp', 'tp')
- rot_grad: float32 [2048, 32], P('sp')
- weight_grad: float32 [512, 1024], P('sp', 'tp')
Inputs may be any that keep to these rules, and one draw needn't show every extreme that they name: `log_sums`: each value lies within one half of log(2048) + 0.5.
All inputs are finite; a program needn't handle non-finite values.
Results may differ from a plain program's by a relative error of at most 0.004.
The roundings to bfloat16 on the way count: a program that leaves them out, or rounds other values in their place, can miss the bound.
Values may be sent and summed in bfloat16 or wider, within the bound.
A program may use at most 64 MiB of HBM per device.

v0:
```python
import functools
import math

import jax
import jax.numpy as jnp
from jax import lax
from jax.experimental import pallas as pl
from jax.experimental.pallas import tpu as pltpu
from jax.sharding import PartitionSpec as P

NOPE = 64
ROPE = 32
VDIM = 64
HEAD = NOPE + ROPE
MESH = pl.DeviceIdType.MESH
F32 = jnp.float32
BF16 = jnp.bfloat16


def dot(x, y, dims):
    return lax.dot_general(x, y, (dims, ((), ())), preferred_element_type=F32)


def three_terms(x):
    hi = x.astype(BF16)
    rest = x - hi.astype(F32)
    mid = rest.astype(BF16)
    low = (rest - mid.astype(F32)).astype(BF16)
    return hi, mid, low


def repeat(start, stop, body):
    if stop - start <= 4:
        for i in range(start, stop):
            body(i)
    else:
        def step(i, carry):
            body(i)
            return carry

        lax.fori_loop(start, stop, step, 0)


def kernel(
    S, TP, H,
    q_in, lat_in, rot_in, w_in, log_in, out_in, go_in,
    qg_ref, kg_ref, vg_ref, rg_ref, wg_ref,
    q_ref, lat_ref, rot_ref, w_ref, log_ref, out_ref, go_ref, loads, ps, pk, wq, kb, lb, ka_ref, va_ref, kat_ref, dk_acc, dv_acc, dq_own, dqs, dqr,
    kvo, kvr, ro, rr, rt, wgs, wgr, qo, qr,
    s1q, r1q, s1k, r1k, s1l, r1l, s2, r2, s3, r3, s4k, r4k, s4r, r4r, s4q, r4q, s5, r5, s6, r6,
):
    G = S // H
    T = q_ref.shape[0]
    half = T // 2
    me = lax.axis_index("sp")
    tpi = lax.axis_index("tp")
    a, b = me // G, lax.rem(me, G)
    scale = HEAD ** (-0.5)

    barrier = pltpu.get_barrier_semaphore()

    def greet(i):
        pl.semaphore_signal(barrier, inc=1, device_id={"sp": lax.rem(me + i, S)}, device_id_type=MESH)

    def greet_tp(i):
        pl.semaphore_signal(barrier, inc=1, device_id={"tp": lax.rem(tpi + i, TP)}, device_id_type=MESH)

    pairs = (
        (q_in, q_ref), (go_in, go_ref), (out_in, out_ref), (log_in, log_ref),
        (lat_in, lat_ref), (w_in, w_ref), (rot_in, rot_ref),
    )
    fetch = [pltpu.make_async_copy(x, y, loads.at[i]) for i, (x, y) in enumerate(pairs)]
    for f in fetch:
        f.start()
    repeat(1, S, greet)
    repeat(1, TP, greet_tp)

    def copy(src, dst, ssem, rsem, sp):
        return pltpu.make_async_remote_copy(
            src_ref=src, dst_ref=dst, send_sem=ssem, recv_sem=rsem,
            device_id={"sp": sp}, device_id_type=MESH,
        )

    for f in fetch[:4]:
        f.wait()
    logs_t = log_ref[...] * math.sqrt(HEAD)
    prod = out_ref[...].astype(F32) * go_ref[...].astype(F32)
    pad = jnp.zeros((T, ROPE - 6), BF16)
    for j in range(H):
        delta = jnp.sum(prod[:, VDIM * j : VDIM * (j + 1)], axis=1, keepdims=True)
        logs = jnp.broadcast_to(logs_t[j : j + 1], (8, T)).T[:, :1]
        terms = three_terms(logs) + three_terms(delta)
        ps[j, :T, :] = jnp.concatenate([q_ref[:, HEAD * j : HEAD * (j + 1)], *terms, pad], axis=1)
        g = go_ref[:, VDIM * j : VDIM * (j + 1)]
        ps[j, T:, :] = jnp.concatenate([g[:half], g[half:]], axis=1)
    wq[b, a] = ps[a]
    pl.semaphore_wait(barrier, S - 1 + TP - 1)

    firsts, lats = [], []
    for d in range(1, H):
        to = lax.rem(a + d, H)
        cq = copy(ps.at[to], wq.at[b, a], s1q.at[d - 1], r1q.at[d - 1], to * G + b)
        ck = copy(pk.at[to], kb.at[a], s1k.at[d - 1], r1k.at[d - 1], to * G + b)
        cq.start()
        firsts.append((cq, ck))

    def relay(d, e):
        src = wq.at[b, lax.rem(a - d + H, H)]
        return copy(src, src, s2.at[e - 1, d], r2.at[e - 1, d], a * G + lax.rem(b + e, G))

    def relay_all(d):
        repeat(1, G, lambda e: relay(d, e).start())

    relay_all(0)
    for f in fetch[4:]:
        f.wait()
    joined = dot(lat_ref[...], w_ref[...], ((1,), (0,))).astype(BF16)
    for j in range(H):
        pk[j, :T, :] = joined[:, 128 * j : 128 * (j + 1)]
        pk[j, T:, :] = rot_ref[...]
    kb[a] = pk[a]
    for d in range(1, H):
        firsts[d - 1][1].start()
    lb[a] = lat_ref[...]
    for d in range(1, H):
        to = lax.rem(a + d, H)
        cl = copy(lat_ref, lb.at[a], s1l.at[d - 1], r1l.at[d - 1], to * G + b)
        cl.start()
        lats.append(cl)
    for d in range(1, H):
        firsts[d - 1][0].wait_recv()
        relay_all(d)
    for d in range(1, H):
        firsts[d - 1][1].wait_recv()

    lane = lax.broadcasted_iota(jnp.int32, (T, ROPE), 1)
    log_ones = jnp.where(lane < 3, -1.0, 0.0).astype(BF16)
    delta_ones = jnp.where((lane >= 3) & (lane < 6), -1.0, 0.0).astype(BF16)
    for j in range(H):
        kv = kb[j, :T, :]
        r = kb[j, T:, :].astype(F32).T.astype(BF16)
        key = jnp.concatenate([kv[:, :NOPE], r, log_ones], axis=1)
        ka_ref[T * j : T * (j + 1), :] = key
        va_ref[T * j : T * (j + 1), :128] = jnp.concatenate([jnp.zeros((T, HEAD), BF16), delta_ones], axis=1)
        va_ref[T * j : T * (j + 1), 128:] = jnp.concatenate([kv[:, NOPE:], jnp.zeros((T, 64), BF16)], axis=1)
        kat_ref[:, T * j : T * (j + 1)] = key.astype(F32).T.astype(BF16)[:HEAD]
    dk_acc[...] = jnp.zeros_like(dk_acc)
    dv_acc[...] = jnp.zeros_like(dv_acc)

    def block(e):
        col = lax.rem(b - e + G, G)
        query = wq[col, :, :T, :].reshape(H * T, 128)
        gp = wq[col, :, T:, :]
        g = jnp.concatenate([gp[:, :, :VDIM], gp[:, :, VDIM:]], axis=1).reshape(H * T, VDIM)
        g = jnp.concatenate([g, jnp.zeros_like(g)], axis=1)
        s = dot(ka_ref[...], query, ((1,), (1,)))
        dp = dot(va_ref[...], jnp.concatenate([query, g], axis=1), ((1,), (1,)))
        p = jnp.exp(s * scale)
        ds = (p * dp).astype(BF16)
        dv_acc[...] += dot(p.astype(BF16), g, ((1,), (0,)))
        dk_acc[...] += dot(ds, query, ((1,), (0,)))
        return dot(kat_ref[...], ds, ((1,), (0,))) * scale

    def part(e):
        return copy(dqs.at[e - 1], dqr.at[e - 1], s3.at[e - 1], r3.at[e - 1], a * G + lax.rem(b - e + G, G))

    dq_own[...] = block(0)

    def other(e):
        for d in range(H):
            relay(d, e).wait_recv()
        dqs[e - 1] = block(e)
        part(e).start()

    repeat(1, G, other)

    dk = dk_acc[...] * scale
    kv = jnp.concatenate([dk[:, :NOPE], dv_acc[:, :VDIM]], axis=1).astype(BF16)
    rot_t = dk.T[NOPE:HEAD]
    for j in range(H):
        kvo[j] = kv[T * j : T * (j + 1)]
        ro[j] = rot_t[:, T * j : T * (j + 1)]
    kvr[a] = kvo[a]
    rr[a] = ro[a]
    backs = []
    for d in range(1, H):
        to = lax.rem(a + d, H)
        ck = copy(kvo.at[to], kvr.at[a], s4k.at[d - 1], r4k.at[d - 1], to * G + b)
        cr = copy(ro.at[to], rr.at[a], s4r.at[d - 1], r4r.at[d - 1], to * G + b)
        cr.start()
        ck.start()
        backs += [ck, cr]

    for cl in lats:
        cl.wait_recv()
    total = None
    lat = lb[...].reshape(H * T, lb.shape[2])
    total = dot(lat, kv, ((0,), (0,)))
    wgs[...] = total.reshape(wgs.shape)
    wgr[me] = wgs[me]

    def share(i):
        to = lax.rem(me + i, S)
        return copy(wgs.at[to], wgr.at[me], s5.at[i - 1], r5.at[i - 1], to)

    repeat(1, S, lambda i: share(i).start())

    def take(e):
        part(e).wait_recv()
        dq_own[...] += dqr[e - 1]

    repeat(1, G, take)
    dq = jnp.concatenate([dq_own[...], jnp.zeros((128 - HEAD, H * T), F32)], axis=0).T.astype(BF16)
    for j in range(H):
        qo[j] = dq[T * j : T * (j + 1)]
    qr[a] = qo[a]
    for d in range(1, H):
        to = lax.rem(a + d, H)
        cq = copy(qo.at[to], qr.at[a], s4q.at[d - 1], r4q.at[d - 1], to * G + b)
        cq.start()
        backs.append(cq)

    for d in range(1, H):
        backs[2 * (d - 1) + 1].wait_recv()
    rt[tpi] = functools.reduce(lambda x, y: x + y, [rr[j] for j in range(H)])

    def swap(i):
        return pltpu.make_async_remote_copy(
            src_ref=rt.at[tpi], dst_ref=rt.at[tpi], send_sem=s6.at[i - 1], recv_sem=r6.at[i - 1],
            device_id={"tp": lax.rem(tpi + i, TP)}, device_id_type=MESH,
        )

    repeat(1, TP, lambda i: swap(i).start())
    for d in range(1, H):
        backs[2 * (d - 1)].wait_recv()
    for j in range(H):
        kg_ref[:, NOPE * j : NOPE * (j + 1)] = kvr[j, :, :NOPE]
        vg_ref[:, VDIM * j : VDIM * (j + 1)] = kvr[j, :, NOPE:]
    repeat(1, TP, lambda i: swap(i).wait_recv())
    rot_sum = functools.reduce(lambda x, y: x + y, [rt[i] for i in range(TP)])
    rg_ref[...] = rot_sum
    repeat(1, S, lambda i: share(i).wait_recv())
    for j in range(H):
        wg_ref[:, 128 * j : 128 * (j + 1)] = functools.reduce(lambda x, y: x + y, [wgr[j * G + i] for i in range(G)])
    for d in range(1, H):
        backs[2 * (H - 1) + d - 1].wait_recv()
    for j in range(H):
        qg_ref[:, HEAD * j : HEAD * (j + 1)] = qr[j, :, :HEAD]

    for cq, ck in firsts:
        cq.wait_send()
        ck.wait_send()
    for c in lats + backs:
        c.wait_send()
    for d in range(H):
        repeat(1, G, lambda e: relay(d, e).wait_send())
    repeat(1, G, lambda e: part(e).wait_send())
    repeat(1, S, lambda i: share(i).wait_send())
    repeat(1, TP, lambda i: swap(i).wait_send())


def put_out(*refs):
    copies = [pltpu.make_async_copy(refs[i], refs[5 + i], refs[10].at[i]) for i in range(5)]
    for c in copies:
        c.start()
    for c in copies:
        c.wait()


def per_device(S, TP, queries, latents, rot_key, kv_weight, log_sums, outputs, out_grad):
    T, rank = latents.shape
    H = log_sums.shape[1]
    G = S // H
    rows = rank // S
    wide = H * T
    dma = lambda *n: pltpu.SemaphoreType.DMA(tuple(max(k, 1) for k in n))
    pairs = lambda *n: [dma(*n), dma(*n)]
    vm = pltpu.VMEM
    g1 = max(G - 1, 1)
    arrays = (queries, latents, rot_key.T, kv_weight, log_sums.T, outputs, out_grad)
    scratch = [
        *[vm(x.shape, x.dtype) for x in arrays], dma(len(arrays)),
        vm((H, T + T // 2, 128), BF16), vm((H, T + ROPE, 128), BF16),
        vm((G, H, T + T // 2, 128), BF16), vm((H, T + ROPE, 128), BF16), vm((H, T, rank), BF16),
        vm((wide, 128), BF16), vm((wide, 256), BF16), vm((HEAD, wide), BF16),
        vm((wide, 128), F32), vm((wide, 128), F32), vm((HEAD, wide), F32),
        vm((g1, HEAD, wide), F32), vm((g1, HEAD, wide), F32),
        vm((H, T, 128), BF16), vm((H, T, 128), BF16), vm((H, ROPE, T), F32), vm((H, ROPE, T), F32),
        vm((TP, ROPE, T), F32), vm((S, rows, 128), F32), vm((S, rows, 128), F32),
        vm((H, T, 128), BF16), vm((H, T, 128), BF16),
        *pairs(H - 1), *pairs(H - 1), *pairs(H - 1), *pairs(G - 1, H), *pairs(G - 1),
        *pairs(H - 1), *pairs(H - 1), *pairs(H - 1), *pairs(S - 1), *pairs(TP - 1),
    ]
    shapes = [
        ((T, H * HEAD), BF16), ((T, H * NOPE), BF16), ((T, H * VDIM), BF16),
        ((ROPE, T), F32), ((rows, H * 128), F32),
    ]
    results = pl.pallas_call(
        functools.partial(kernel, S, TP, H),
        out_shape=[pltpu.VMEM(*x) for x in shapes],
        in_specs=[pl.BlockSpec(memory_space=pltpu.HBM)] * 7,
        out_specs=[pl.BlockSpec(memory_space=vm)] * 5,
        scratch_shapes=scratch,
        compiler_params=pltpu.CompilerParams(
            collective_id=0, has_side_effects=True, vmem_limit_bytes=50000 * 1024
        ),
    )(*arrays)
    query_grad, key_grad, value_grad, rot_grad, weight_grad = pl.pallas_call(
        put_out,
        out_shape=[jax.ShapeDtypeStruct(*x) for x in shapes],
        in_specs=[pl.BlockSpec(memory_space=vm)] * 5,
        out_specs=[pl.BlockSpec(memory_space=pltpu.HBM)] * 5,
        scratch_shapes=[dma(5)],
    )(*results)
    return query_grad, key_grad, value_grad, rot_grad.T, weight_grad


def solution(mesh):
    placed = (
        P("sp", "tp"), P("sp", None), P("sp", None), P(None, "tp"),
        P("sp", "tp"), P("sp", "tp"), P("sp", "tp"),
    )
    return jax.shard_map(
        functools.partial(per_device, mesh.shape["sp"], mesh.shape["tp"]),
        mesh=mesh,
        in_specs=placed,
        out_specs=(P("sp", "tp"), P("sp", "tp"), P("sp", "tp"), P("sp", None), P("sp", "tp")),
        check_vma=False,
    )
```

profile of v0, /device:TPU:0, one launch (start us, length us, event | category | flops | bytes accessed | tf_op | source)
XLA Modules:
  0.0 52.3 jit_solution(5596342097745087996)
XLA Ops:
  0.6 0.0 copy-start.11
  0.6 0.7 %copy-done.11 = f32[128,4]{0,1:T(4,128)S(1)} copy-done((f32[128,4]{0,1:T(4,128)S(1)}, f32[128,4]{0,1:T(4,128)}, u32[]{:S(2)}) %copy-start.11) | copy-done | bytes 2072
  1.3 0.0 copy-start
  1.3 1.0 %copy-done = bf16[512,512]{1,0:T(8,128)(2,1)S(1)} copy-done((bf16[512,512]{1,0:T(8,128)(2,1)S(1)}, bf16[512,512]{1,0:T(8,128)(2,1)}, u32[]{:S(2)}) %copy-start) | copy-done | bytes 524312
  2.4 0.0 copy-start.1
  2.4 0.9 %copy-done.1 = bf16[128,512]{1,0:T(8,128)(2,1)S(1)} copy-done((bf16[128,512]{1,0:T(8,128)(2,1)S(1)}, bf16[128,512]{1,0:T(8,128)(2,1)}, u32[]{:S(2)}) %copy-start.1) | copy-done | bytes 131096
  3.3 0.0 copy-start.2
  3.3 0.9 %copy-done.2 = bf16[128,384]{1,0:T(8,128)(2,1)S(1)} copy-done((bf16[128,384]{1,0:T(8,128)(2,1)S(1)}, bf16[128,384]{1,0:T(8,128)(2,1)}, u32[]{:S(2)}) %copy-start.2) | copy-done | bytes 98328
  4.2 0.0 copy-start.4
  4.2 0.8 %copy-done.4 = bf16[128,256]{1,0:T(8,128)(2,1)S(1)} copy-done((bf16[128,256]{1,0:T(8,128)(2,1)S(1)}, bf16[128,256]{1,0:T(8,128)(2,1)}, u32[]{:S(2)}) %copy-start.4) | copy-done | bytes 65560
  5.0 0.0 copy-start.5
  5.0 0.8 %copy-done.5 = bf16[128,256]{1,0:T(8,128)(2,1)S(1)} copy-done((bf16[128,256]{1,0:T(8,128)(2,1)S(1)}, bf16[128,256]{1,0:T(8,128)(2,1)}, u32[]{:S(2)}) %copy-start.5) | copy-done | bytes 65560
  5.8 0.0 copy-start.10
  5.8 0.7 %copy-done.10 = bf16[128,32]{0,1:T(8,128)(2,1)S(1)} copy-done((bf16[128,32]{0,1:T(8,128)(2,1)S(1)}, bf16[128,32]{0,1:T(8,128)(2,1)}, u32[]{:S(2)}) %copy-start.10) | copy-done | bytes 8216
  6.5 41.0 %shard_map.110 = (bf16[128,384]{1,0:T(8,128)(2,1)S(1)}, bf16[128,256]{1,0:T(8,128)(2,1)S(1)}, bf16[128,256]{1,0:T(8,128)(2,1)S(1)}, f32[32,128]{1,0:T(8,128)S(1)}, f32[32,512]{1,0:T(8,128)S(1)}) custom-call(bf16[128,384]{1,0:T(8,128)(2,1)S(1)} %copy-done.2, bf16[128,512]{1,0:T(8,128)(2,1)S(1)} %copy-done.1, bf16[32,128]{1,0:T(8,128)(2,1)S(1)} %bitcast.3, ...), custom_call_target="tpu_custom_call" | custom-call | tf_op jit(solution)/shard_map/pallas_call | solution.py:298
  47.5 0.0 copy-start.3
  47.5 0.6 %copy-done.3 = bf16[128,384]{1,0:T(8,128)(2,1)} copy-done((bf16[128,384]{1,0:T(8,128)(2,1)}, bf16[128,384]{1,0:T(8,128)(2,1)S(1)}, u32[]{:S(2)}) %copy-start.3) | copy-done | bytes 98328
  48.1 0.0 copy-start.6
  48.1 0.6 %copy-done.6 = bf16[128,256]{1,0:T(8,128)(2,1)} copy-done((bf16[128,256]{1,0:T(8,128)(2,1)}, bf16[128,256]{1,0:T(8,128)(2,1)S(1)}, u32[]{:S(2)}) %copy-start.6) | copy-done | bytes 65560
  48.8 0.0 copy-start.7
  48.8 0.6 %copy-done.7 = bf16[128,256]{1,0:T(8,128)(2,1)} copy-done((bf16[128,256]{1,0:T(8,128)(2,1)}, bf16[128,256]{1,0:T(8,128)(2,1)S(1)}, u32[]{:S(2)}) %copy-start.7) | copy-done | bytes 65560
  49.4 0.0 copy-start.8
  49.4 0.6 %copy-done.8 = f32[32,512]{1,0:T(8,128)} copy-done((f32[32,512]{1,0:T(8,128)}, f32[32,512]{1,0:T(8,128)S(1)}, u32[]{:S(2)}) %copy-start.8) | copy-done | bytes 65560
  50.0 0.0 copy-start.9
  50.0 0.6 %copy-done.9 = f32[32,128]{1,0:T(8,128)} copy-done((f32[32,128]{1,0:T(8,128)}, f32[32,128]{1,0:T(8,128)S(1)}, u32[]{:S(2)}) %copy-start.9) | copy-done | bytes 16408
  50.6 1.7 %shard_map.111 = (bf16[128,384]{1,0:T(8,128)(2,1)}, bf16[128,256]{1,0:T(8,128)(2,1)}, bf16[128,256]{1,0:T(8,128)(2,1)}, f32[32,128]{1,0:T(8,128)}, f32[32,512]{1,0:T(8,128)}) custom-call(bf16[128,384]{1,0:T(8,128)(2,1)} %copy-done.3, bf16[128,256]{1,0:T(8,128)(2,1)} %copy-done.6, bf16[128,256]{1,0:T(8,128)(2,1)} %copy-done.7, f32[32,128]{1,0:T(8,128)} %copy-done.9, ...), custom_call_target="tpu_custom_call" | custom-call | tf_op jit(solution)/shard_map/pallas_call | solution.py:308
Async XLA Ops:
  0.6 0.7 %copy-start.11 = (f32[128,4]{0,1:T(4,128)S(1)}, f32[128,4]{0,1:T(4,128)}, u32[]{:S(2)}) copy-start(f32[128,4]{0,1:T(4,128)} %param.11) | copy-start | bytes 6148
  1.3 1.0 %copy-start = (bf16[512,512]{1,0:T(8,128)(2,1)S(1)}, bf16[512,512]{1,0:T(8,128)(2,1)}, u32[]{:S(2)}) copy-start(bf16[512,512]{1,0:T(8,128)(2,1)} %w_in.1) | copy-start | bytes 1572868
  2.4 0.9 %copy-start.1 = (bf16[128,512]{1,0:T(8,128)(2,1)S(1)}, bf16[128,512]{1,0:T(8,128)(2,1)}, u32[]{:S(2)}) copy-start(bf16[128,512]{1,0:T(8,128)(2,1)} %lat_in.1) | copy-start | bytes 393220
  3.3 0.9 %copy-start.2 = (bf16[128,384]{1,0:T(8,128)(2,1)S(1)}, bf16[128,384]{1,0:T(8,128)(2,1)}, u32[]{:S(2)}) copy-start(bf16[128,384]{1,0:T(8,128)(2,1)} %q_in.1) | copy-start | bytes 294916
  4.2 0.8 %copy-start.4 = (bf16[128,256]{1,0:T(8,128)(2,1)S(1)}, bf16[128,256]{1,0:T(8,128)(2,1)}, u32[]{:S(2)}) copy-start(bf16[128,256]{1,0:T(8,128)(2,1)} %out_in.1) | copy-start | bytes 196612
  5.0 0.8 %copy-start.5 = (bf16[128,256]{1,0:T(8,128)(2,1)S(1)}, bf16[128,256]{1,0:T(8,128)(2,1)}, u32[]{:S(2)}) copy-start(bf16[128,256]{1,0:T(8,128)(2,1)} %go_in.1) | copy-start | bytes 196612
  5.8 0.7 %copy-start.10 = (bf16[128,32]{0,1:T(8,128)(2,1)S(1)}, bf16[128,32]{0,1:T(8,128)(2,1)}, u32[]{:S(2)}) copy-start(bf16[128,32]{0,1:T(8,128)(2,1)} %param.9) | copy-start | bytes 24580
  47.5 0.6 %copy-start.3 = (bf16[128,384]{1,0:T(8,128)(2,1)}, bf16[128,384]{1,0:T(8,128)(2,1)S(1)}, u32[]{:S(2)}) copy-start(bf16[128,384]{1,0:T(8,128)(2,1)S(1)} %get-tuple-element.15.refs_0_) | copy-start | bytes 294916
  48.1 0.6 %copy-start.6 = (bf16[128,256]{1,0:T(8,128)(2,1)}, bf16[128,256]{1,0:T(8,128)(2,1)S(1)}, u32[]{:S(2)}) copy-start(bf16[128,256]{1,0:T(8,128)(2,1)S(1)} %get-tuple-element.16.refs_1_) | copy-start | bytes 196612
  48.8 0.6 %copy-start.7 = (bf16[128,256]{1,0:T(8,128)(2,1)}, bf16[128,256]{1,0:T(8,128)(2,1)S(1)}, u32[]{:S(2)}) copy-start(bf16[128,256]{1,0:T(8,128)(2,1)S(1)} %get-tuple-element.17.refs_2_) | copy-start | bytes 196612
  49.4 0.6 %copy-start.8 = (f32[32,512]{1,0:T(8,128)}, f32[32,512]{1,0:T(8,128)S(1)}, u32[]{:S(2)}) copy-start(f32[32,512]{1,0:T(8,128)S(1)} %get-tuple-element.19.refs_4_) | copy-start | bytes 196612
  50.0 0.6 %copy-start.9 = (f32[32,128]{1,0:T(8,128)}, f32[32,128]{1,0:T(8,128)S(1)}, u32[]{:S(2)}) copy-start(f32[32,128]{1,0:T(8,128)S(1)} %get-tuple-element.18.refs_3_) | copy-start | bytes 49156
where the time goes:
time: 52.7 us; the launch traced here: 52.3 us
  Pallas kernels  42.7 us (81%)
  local copies, waits for them, and re-layouts  8.96 us (17%)
  between operations  0.67 us (1%)
    pallas_call x1, Pallas kernels, per_device(): pl.pallas_call(functools.partial(kernel, S, TP, H), out_shape=[pltpu.VMEM...  41 us
    unnamed x24, local copies, waits for them, and re-layouts  8.96 us
    pallas_call x1, Pallas kernels, per_device(): pl.pallas_call(put_out, out_shape=[jax.ShapeDtypeStruct(*x) for x in shap...  1.72 us

commit v1 on v0

--- a/solution.py
+++ b/solution.py
@@ -12,6 +12,8 @@
 ROPE = 32
 VDIM = 64
 HEAD = NOPE + ROPE
+VMEM_BYTES = 67043328
+SPARE = 8192
 MESH = pl.DeviceIdType.MESH
 F32 = jnp.float32
 BF16 = jnp.bfloat16
@@ -46,8 +48,8 @@
     q_in, lat_in, rot_in, w_in, log_in, out_in, go_in,
     qg_ref, kg_ref, vg_ref, rg_ref, wg_ref,
     q_ref, lat_ref, rot_ref, w_ref, log_ref, out_ref, go_ref, loads, ps, pk, wq, kb, lb, ka_ref, va_ref, kat_ref, dk_acc, dv_acc, dq_own, dqs, dqr,
-    kvo, kvr, ro, rr, rt, wgs, wgr, qo, qr,
-    s1q, r1q, s1k, r1k, s1l, r1l, s2, r2, s3, r3, s4k, r4k, s4r, r4r, s4q, r4q, s5, r5, s6, r6,
+    kvo, kvr, ro, rr, rt, wgs, wgr, wh, wo, qo, qr,
+    s1q, r1q, s1k, r1k, s1l, r1l, s2, r2, s3, r3, s4k, r4k, s4r, r4r, s4q, r4q, s5, r5, s6, r6, s7, r7,
 ):
     G = S // H
     T = q_ref.shape[0]
@@ -147,7 +149,7 @@
     dk_acc[...] = jnp.zeros_like(dk_acc)
     dv_acc[...] = jnp.zeros_like(dv_acc)
 
-    def block(e):
+    def block(e, keep):
         col = lax.rem(b - e + G, G)
         query = wq[col, :, :T, :].reshape(H * T, 128)
         gp = wq[col, :, T:, :]
@@ -157,20 +159,27 @@
         dp = dot(va_ref[...], jnp.concatenate([query, g], axis=1), ((1,), (1,)))
         p = jnp.exp(s * scale)
         ds = (p * dp).astype(BF16)
+        keep(dot(kat_ref[...], ds, ((1,), (0,))) * scale)
         dv_acc[...] += dot(p.astype(BF16), g, ((1,), (0,)))
         dk_acc[...] += dot(ds, query, ((1,), (0,)))
-        return dot(kat_ref[...], ds, ((1,), (0,))) * scale
 
     def part(e):
         return copy(dqs.at[e - 1], dqr.at[e - 1], s3.at[e - 1], r3.at[e - 1], a * G + lax.rem(b - e + G, G))
 
-    dq_own[...] = block(0)
+    def keep_own(x):
+        dq_own[...] = x
+
+    block(0, keep_own)
 
     def other(e):
         for d in range(H):
             relay(d, e).wait_recv()
-        dqs[e - 1] = block(e)
-        part(e).start()
+
+        def send(x):
+            dqs[e - 1] = x
+            part(e).start()
+
+        block(e, send)
 
     repeat(1, G, other)
 
@@ -193,17 +202,19 @@
 
     for cl in lats:
         cl.wait_recv()
-    total = None
     lat = lb[...].reshape(H * T, lb.shape[2])
     total = dot(lat, kv, ((0,), (0,)))
-    wgs[...] = total.reshape(wgs.shape)
-    wgr[me] = wgs[me]
-
-    def share(i):
-        to = lax.rem(me + i, S)
-        return copy(wgs.at[to], wgr.at[me], s5.at[i - 1], r5.at[i - 1], to)
-
-    repeat(1, S, lambda i: share(i).start())
+    rows = wgs.shape[2]
+    for i in range(G):
+        for j in range(H):
+            wgs[i, j] = total[(j * G + i) * rows : (j * G + i + 1) * rows]
+    wgr[b] = wgs[b]
+
+    def share(e):
+        to = lax.rem(b + e, G)
+        return copy(wgs.at[to], wgr.at[b], s5.at[e - 1], r5.at[e - 1], a * G + to)
+
+    repeat(1, G, lambda e: share(e).start())
 
     def take(e):
         part(e).wait_recv()
@@ -220,6 +231,15 @@
         cq.start()
         backs.append(cq)
 
+    repeat(1, G, lambda e: share(e).wait_recv())
+    wh[...] = functools.reduce(lambda x, y: x + y, [wgr[i] for i in range(G)])
+    wo[a] = wh[a]
+    lasts = []
+    for d in range(1, H):
+        to = lax.rem(a + d, H)
+        c = copy(wh.at[to], wo.at[a], s7.at[d - 1], r7.at[d - 1], to * G + b)
+        c.start()
+        lasts.append(c)
     for d in range(1, H):
         backs[2 * (d - 1) + 1].wait_recv()
     rt[tpi] = functools.reduce(lambda x, y: x + y, [rr[j] for j in range(H)])
@@ -239,23 +259,25 @@
     repeat(1, TP, lambda i: swap(i).wait_recv())
     rot_sum = functools.reduce(lambda x, y: x + y, [rt[i] for i in range(TP)])
     rg_ref[...] = rot_sum
-    repeat(1, S, lambda i: share(i).wait_recv())
-    for j in range(H):
-        wg_ref[:, 128 * j : 128 * (j + 1)] = functools.reduce(lambda x, y: x + y, [wgr[j * G + i] for i in range(G)])
     for d in range(1, H):
         backs[2 * (H - 1) + d - 1].wait_recv()
     for j in range(H):
         qg_ref[:, HEAD * j : HEAD * (j + 1)] = qr[j, :, :HEAD]
+
+    for c in lasts:
+        c.wait_recv()
+    for j in range(H):
+        wg_ref[:, 128 * j : 128 * (j + 1)] = wo[j]
 
     for cq, ck in firsts:
         cq.wait_send()
         ck.wait_send()
-    for c in lats + backs:
+    for c in lats + backs + lasts:
         c.wait_send()
     for d in range(H):
         repeat(1, G, lambda e: relay(d, e).wait_send())
     repeat(1, G, lambda e: part(e).wait_send())
-    repeat(1, S, lambda i: share(i).wait_send())
+    repeat(1, G, lambda e: share(e).wait_send())
     repeat(1, TP, lambda i: swap(i).wait_send())
 
 
@@ -286,15 +308,16 @@
         vm((wide, 128), F32), vm((wide, 128), F32), vm((HEAD, wide), F32),
         vm((g1, HEAD, wide), F32), vm((g1, HEAD, wide), F32),
         vm((H, T, 128), BF16), vm((H, T, 128), BF16), vm((H, ROPE, T), F32), vm((H, ROPE, T), F32),
-        vm((TP, ROPE, T), F32), vm((S, rows, 128), F32), vm((S, rows, 128), F32),
+        vm((TP, ROPE, T), F32), *[vm((G, H, rows, 128), F32)] * 2, *[vm((H, rows, 128), F32)] * 2,
         vm((H, T, 128), BF16), vm((H, T, 128), BF16),
         *pairs(H - 1), *pairs(H - 1), *pairs(H - 1), *pairs(G - 1, H), *pairs(G - 1),
-        *pairs(H - 1), *pairs(H - 1), *pairs(H - 1), *pairs(S - 1), *pairs(TP - 1),
+        *pairs(H - 1), *pairs(H - 1), *pairs(H - 1), *pairs(G - 1), *pairs(TP - 1), *pairs(H - 1),
     ]
     shapes = [
         ((T, H * HEAD), BF16), ((T, H * NOPE), BF16), ((T, H * VDIM), BF16),
         ((ROPE, T), F32), ((rows, H * 128), F32),
     ]
+    held = sum(x[0] * -(-x[1] // 128) * 128 * jnp.dtype(t).itemsize for x, t in shapes)
     results = pl.pallas_call(
         functools.partial(kernel, S, TP, H),
         out_shape=[pltpu.VMEM(*x) for x in shapes],
@@ -302,7 +325,7 @@
         out_specs=[pl.BlockSpec(memory_space=vm)] * 5,
         scratch_shapes=scratch,
         compiler_params=pltpu.CompilerParams(
-            collective_id=0, has_side_effects=True, vmem_limit_bytes=50000 * 1024
+            collective_id=0, has_side_effects=True, vmem_limit_bytes=VMEM_BYTES - held - SPARE
         ),
     )(*arrays)
     query_grad, key_grad, value_grad, rot_grad, weight_grad = pl.pallas_call(
@@ -311,6 +334,7 @@
         in_specs=[pl.BlockSpec(memory_space=vm)] * 5,
         out_specs=[pl.BlockSpec(memory_space=pltpu.HBM)] * 5,
         scratch_shapes=[dma(5)],
+        compiler_params=pltpu.CompilerParams(vmem_limit_bytes=1 << 20),
     )(*results)
     return query_grad, key_grad, value_grad, rot_grad.T, weight_grad
 

time: 52.7 us -> 40.6 us (0.77)
  local copies, waits for them, and re-layouts: 8.96 us -> 0 us
  Pallas kernels: 42.7 us -> 39.8 us
    unnamed x24 -> x0, local copies, waits for them, and re-layouts: 8.96 us -> none
    pallas_call x1, Pallas kernels: 41 us -> 39 us  [per_device(): pl.pallas_call(functools.partial(kernel, S, TP, H), out_shape=[pltpu.VMEM...]
    pallas_call x1, Pallas kernels: 1.72 us -> 0.76 us  [per_device(): pl.pallas_call(put_out, out_shape=[jax.ShapeDtypeStruct(*x) for x in shap...]
where the time goes in v1:
time: 40.6 us; the launch traced here: 40.4 us
  Pallas kernels  39.8 us (98%)
  between operations  0.64 us (2%)
    pallas_call x1, Pallas kernels, per_device(): pl.pallas_call(functools.partial(kernel, S, TP, H), out_shape=[pltpu.VMEM...  39 us

profile of v1, /device:TPU:0, one launch (start us, length us, event | category | flops | bytes accessed | tf_op | source)
XLA Modules:
  0.0 40.4 jit_solution(6536037475693025685)
XLA Ops:
  0.6 39.0 %shard_map.110 = (bf16[128,384]{1,0:T(8,128)(2,1)S(1)}, bf16[128,256]{1,0:T(8,128)(2,1)S(1)}, bf16[128,256]{1,0:T(8,128)(2,1)S(1)}, f32[32,128]{1,0:T(8,128)S(1)}, f32[32,512]{1,0:T(8,128)S(1)}) custom-call(bf16[128,384]{1,0:T(8,128)(2,1)} %q_in.1, bf16[128,512]{1,0:T(8,128)(2,1)} %lat_in.1, bf16[32,128]{1,0:T(8,128)(2,1)} %bitcast.3, ...), custom_call_target="tpu_custom_call" | custom-call | tf_op jit(solution)/shard_map/pallas_call | solution.py:321
  39.7 0.8 %shard_map.111 = (bf16[128,384]{1,0:T(8,128)(2,1)}, bf16[128,256]{1,0:T(8,128)(2,1)}, bf16[128,256]{1,0:T(8,128)(2,1)}, f32[32,128]{1,0:T(8,128)}, f32[32,512]{1,0:T(8,128)}) custom-call(bf16[128,384]{1,0:T(8,128)(2,1)S(1)} %get-tuple-element.15.refs_0_, bf16[128,256]{1,0:T(8,128)(2,1)S(1)} %get-tuple-element.16.refs_1_, ...), custom_call_target="tpu_custom_call" | custom-call | tf_op jit(solution)/shard_map/pallas_call | solution.py:331

commit v2 on v1

--- a/solution.py
+++ b/solution.py
@@ -49,7 +49,7 @@
     qg_ref, kg_ref, vg_ref, rg_ref, wg_ref,
     q_ref, lat_ref, rot_ref, w_ref, log_ref, out_ref, go_ref, loads, ps, pk, wq, kb, lb, ka_ref, va_ref, kat_ref, dk_acc, dv_acc, dq_own, dqs, dqr,
     kvo, kvr, ro, rr, rt, wgs, wgr, wh, wo, qo, qr,
-    s1q, r1q, s1k, r1k, s1l, r1l, s2, r2, s3, r3, s4k, r4k, s4r, r4r, s4q, r4q, s5, r5, s6, r6, s7, r7,
+    s1q, r1q, s1k, r1k, s1l, r1l, s2, r2, s3, r3, s4k, r4k, s4r, r4r, s4q, r4q, s5, r5, s6, r6, s7, r7, s8, r8,
 ):
     G = S // H
     T = q_ref.shape[0]
@@ -123,10 +123,12 @@
     kb[a] = pk[a]
     for d in range(1, H):
         firsts[d - 1][1].start()
-    lb[a] = lat_ref[...]
-    for d in range(1, H):
-        to = lax.rem(a + d, H)
-        cl = copy(lat_ref, lb.at[a], s1l.at[d - 1], r1l.at[d - 1], to * G + b)
+    lb[a] = lat_ref[...].reshape(lb.shape[1:])
+    slab = T // TP
+    mine = lat_ref.at[pl.ds(pl.multiple_of(tpi * slab, slab), slab)]
+    for d in range(1, H):
+        to = lax.rem(a + d, H)
+        cl = copy(mine, lb.at[a, tpi], s1l.at[d - 1], r1l.at[d - 1], to * G + b)
         cl.start()
         lats.append(cl)
     for d in range(1, H):
@@ -181,7 +183,18 @@
 
         block(e, send)
 
-    repeat(1, G, other)
+    def hand_on(d, i):
+        piece = lb.at[lax.rem(a - d + H, H), tpi]
+        return pltpu.make_async_remote_copy(
+            src_ref=piece, dst_ref=piece, send_sem=s8.at[d - 1, i - 1], recv_sem=r8.at[d - 1, i - 1],
+            device_id={"tp": lax.rem(tpi + i, TP)}, device_id_type=MESH,
+        )
+
+    repeat(1, min(3, G), other)
+    for d in range(1, H):
+        lats[d - 1].wait_recv()
+        repeat(1, TP, lambda i: hand_on(d, i).start())
+    repeat(min(3, G), G, other)
 
     dk = dk_acc[...] * scale
     kv = jnp.concatenate([dk[:, :NOPE], dv_acc[:, :VDIM]], axis=1).astype(BF16)
@@ -200,9 +213,9 @@
         ck.start()
         backs += [ck, cr]
 
-    for cl in lats:
-        cl.wait_recv()
-    lat = lb[...].reshape(H * T, lb.shape[2])
+    for d in range(1, H):
+        repeat(1, TP, lambda i: hand_on(d, i).wait_recv())
+    lat = lb[...].reshape(H * T, lb.shape[3])
     total = dot(lat, kv, ((0,), (0,)))
     rows = wgs.shape[2]
     for i in range(G):
@@ -279,6 +292,8 @@
     repeat(1, G, lambda e: part(e).wait_send())
     repeat(1, G, lambda e: share(e).wait_send())
     repeat(1, TP, lambda i: swap(i).wait_send())
+    for d in range(1, H):
+        repeat(1, TP, lambda i: hand_on(d, i).wait_send())
 
 
 def put_out(*refs):
@@ -303,7 +318,7 @@
     scratch = [
         *[vm(x.shape, x.dtype) for x in arrays], dma(len(arrays)),
         vm((H, T + T // 2, 128), BF16), vm((H, T + ROPE, 128), BF16),
-        vm((G, H, T + T // 2, 128), BF16), vm((H, T + ROPE, 128), BF16), vm((H, T, rank), BF16),
+        vm((G, H, T + T // 2, 128), BF16), vm((H, T + ROPE, 128), BF16), vm((H, TP, T // TP, rank), BF16),
         vm((wide, 128), BF16), vm((wide, 256), BF16), vm((HEAD, wide), BF16),
         vm((wide, 128), F32), vm((wide, 128), F32), vm((HEAD, wide), F32),
         vm((g1, HEAD, wide), F32), vm((g1, HEAD, wide), F32),
@@ -311,7 +326,7 @@
         vm((TP, ROPE, T), F32), *[vm((G, H, rows, 128), F32)] * 2, *[vm((H, rows, 128), F32)] * 2,
         vm((H, T, 128), BF16), vm((H, T, 128), BF16),
         *pairs(H - 1), *pairs(H - 1), *pairs(H - 1), *pairs(G - 1, H), *pairs(G - 1),
-        *pairs(H - 1), *pairs(H - 1), *pairs(H - 1), *pairs(G - 1), *pairs(TP - 1), *pairs(H - 1),
+        *pairs(H - 1), *pairs(H - 1), *pairs(H - 1), *pairs(G - 1), *pairs(TP - 1), *pairs(H - 1), *pairs(H - 1, TP - 1),
     ]
     shapes = [
         ((T, H * HEAD), BF16), ((T, H * NOPE), BF16), ((T, H * VDIM), BF16),

time: 40.6 us -> 38.8 us (0.956)
  Pallas kernels: 39.8 us -> 38 us
    pallas_call x1, Pallas kernels: 39 us -> 37.2 us  [per_device(): pl.pallas_call(functools.partial(kernel, S, TP, H), out_shape=[pltpu.VMEM...]
where the time goes in v2:
time: 38.8 us; the launch traced here: 38.6 us
  Pallas kernels  38 us (98%)
  between operations  0.64 us (2%)
    pallas_call x1, Pallas kernels, per_device(): pl.pallas_call(functools.partial(kernel, S, TP, H), out_shape=[pltpu.VMEM...  37.2 us

profile of v2, /device:TPU:0, one launch (start us, length us, event | category | flops | bytes accessed | tf_op | source)
XLA Modules:
  0.0 38.6 jit_solution(5787247381838307675)
XLA Ops:
  0.6 37.2 %shard_map.110 = (bf16[128,384]{1,0:T(8,128)(2,1)S(1)}, bf16[128,256]{1,0:T(8,128)(2,1)S(1)}, bf16[128,256]{1,0:T(8,128)(2,1)S(1)}, f32[32,128]{1,0:T(8,128)S(1)}, f32[32,512]{1,0:T(8,128)S(1)}) custom-call(bf16[128,384]{1,0:T(8,128)(2,1)} %q_in.1, bf16[128,512]{1,0:T(8,128)(2,1)} %lat_in.1, bf16[32,128]{1,0:T(8,128)(2,1)} %bitcast.3, ...), custom_call_target="tpu_custom_call" | custom-call | tf_op jit(solution)/shard_map/pallas_call | solution.py:336
  37.9 0.8 %shard_map.111 = (bf16[128,384]{1,0:T(8,128)(2,1)}, bf16[128,256]{1,0:T(8,128)(2,1)}, bf16[128,256]{1,0:T(8,128)(2,1)}, f32[32,128]{1,0:T(8,128)}, f32[32,512]{1,0:T(8,128)}) custom-call(bf16[128,384]{1,0:T(8,128)(2,1)S(1)} %get-tuple-element.15.refs_0_, bf16[128,256]{1,0:T(8,128)(2,1)S(1)} %get-tuple-element.16.refs_1_, ...), custom_call_target="tpu_custom_call" | custom-call | tf_op jit(solution)/shard_map/pallas_call | solution.py:346
